TPU v7x, 32 devices: a whole 2x2x4 slice. The times are simulated.
32 devices in a mesh: sp: 8 (over z, y), tp: 4 (over x, core).
Axes of the slice: x: 2, y: 2, z: 4, core: 2. Of those that a mesh axis runs over, the one named last changes fastest.
Arguments:
- queries: bfloat16 [2048, 2048], P('sp', 'tp'), may hold values from -6 to 6
- keys: bfloat16 [2048, 512], P('sp', 'tp'), may hold values from -6 to 6
- values: bfloat16 [2048, 512], P('sp', 'tp'), may hold values from -6 to 6
- query_gain: float32 [64], replicated, may hold values from 0.8 to 5
- key_gain: float32 [64], replicated, may hold values from 0.8 to 5
- stream: bfloat16 [2048, 2048], P('sp'), may hold values from -0.1796875 to 0.1796875
- out_weight: bfloat16 [2048, 2048], P('tp'), may hold values from -0.125 to 0.125
- mixer_gain: float32 [2048], replicated, may hold values from 0.1 to 1.9
- up_weight: bfloat16 [2048, 8192], P('sp', 'tp'), may hold values from -0.125 to 0.125
- down_weight: bfloat16 [8192, 2048], P('tp', 'sp'), may hold values from -0.0625 to 0.0625
Outputs:
- updated: bfloat16 [2048, 2048], P('sp', 'tp')
All inputs are finite; a program needn't handle non-finite values.
Results may differ from a plain program's by a relative error of at most 0.02.
The roundings to bfloat16 on the way count: a program that leaves them out, or rounds other values in their place, can miss the bound.
Values may be sent and summed in bfloat16 or wider, within the bound.
A program may use at most 128 MiB of HBM per device.

v0:
```python
import math
import jax
import jax.numpy as jnp
from jax import lax
from jax.sharding import PartitionSpec as P

HD = 64
GRID_W = 64
EPSILON = 1e-06


def prepare(projected, gain_vec, offset):
    row_count = projected.shape[0]
    head_count = projected.shape[1] // HD
    widened = projected.astype(jnp.float32).reshape(row_count, head_count, HD)
    widened = (
        widened
        * lax.rsqrt(jnp.mean(widened * widened, axis=-1, keepdims=True) + EPSILON)
        * gain_vec
    )
    position = offset + jnp.arange(row_count, dtype=jnp.int32)
    grid_row = (position // GRID_W).astype(jnp.float32)
    grid_col = (position % GRID_W).astype(jnp.float32)
    half_dim = HD // 2
    inverse = 1.0 / jnp.power(10000.0, jnp.arange(0, half_dim, 2, dtype=jnp.float32) / half_dim)
    angle = jnp.concatenate([grid_row[:, None] * inverse, grid_col[:, None] * inverse], axis=-1)
    cosine = jnp.cos(angle)[:, None, :]
    sine_table = jnp.sin(angle)[:, None, :]
    paired = widened.reshape(row_count, head_count, half_dim, 2)
    former = paired[..., 0]
    latter = paired[..., 1]
    rotated = jnp.stack(
        [former * cosine - latter * sine_table, former * sine_table + latter * cosine], axis=-1
    )
    return rotated.reshape(row_count, head_count, HD).astype(jnp.bfloat16)


def attend_block(state, grouped, key_block, value_block):
    running, totals, weighted = state
    scores = jnp.einsum("qhgd,khd->hgqk", grouped, key_block, preferred_element_type=jnp.float32)
    scores = scores * (1.0 / math.sqrt(HD))
    newest = jnp.maximum(running, jnp.max(scores, axis=-1))
    rescale = jnp.exp(running - newest)
    exps = jnp.exp(scores - newest[..., None])
    totals = totals * rescale + jnp.sum(exps, axis=-1)
    weighted = weighted * rescale[..., None] + jnp.einsum(
        "hgqk,khd->hgqd", exps.astype(jnp.bfloat16), value_block, preferred_element_type=jnp.float32
    )
    return (newest, totals, weighted)


def shards(
    queries,
    keys,
    values,
    query_gain,
    key_gain,
    stream,
    out_weight,
    mixer_gain,
    up_weight,
    down_weight,
):
    local_rows = queries.shape[0]
    offset = lax.axis_index("sp") * local_rows
    kv_count = keys.shape[1] // HD
    group_size = queries.shape[1] // HD // kv_count
    grouped = prepare(queries, query_gain, offset).reshape(local_rows, kv_count, group_size, HD)
    prepared_keys = prepare(keys, key_gain, offset).reshape(local_rows, kv_count * HD)
    initial = (
        jnp.full((kv_count, group_size, local_rows), -1e30, jnp.float32),
        jnp.zeros((kv_count, group_size, local_rows), jnp.float32),
        jnp.zeros((kv_count, group_size, local_rows, HD), jnp.float32),
    )
    key_rows = lax.all_gather(prepared_keys, "sp", axis=0, tiled=True)
    value_rows = lax.all_gather(values, "sp", axis=0, tiled=True)
    piece_rows = key_rows.shape[0]
    block_rows = piece_rows if piece_rows <= 2048 else math.gcd(piece_rows, 2048)
    key_blocks = key_rows.reshape(piece_rows // block_rows, block_rows, kv_count, HD)
    value_blocks = value_rows.reshape(piece_rows // block_rows, block_rows, kv_count, HD)

    def visit_block(block_index, state_now):
        return attend_block(state_now, grouped, key_blocks[block_index], value_blocks[block_index])

    running, totals, weighted = lax.fori_loop(0, piece_rows // block_rows, visit_block, initial)
    head_out = weighted / totals[..., None]
    head_out = jnp.transpose(head_out, (2, 0, 1, 3)).reshape(local_rows, -1).astype(jnp.bfloat16)
    partial_value = jnp.dot(head_out, out_weight, preferred_element_type=jnp.float32)
    model_width = partial_value.shape[1]
    share_cols = model_width // lax.axis_size("tp")
    first_col = lax.axis_index("tp") * share_cols
    summed = lax.psum(partial_value.astype(jnp.bfloat16), "tp").astype(jnp.float32)
    mid = (stream.astype(jnp.float32) + summed).astype(jnp.bfloat16)
    mid_wide = mid.astype(jnp.float32)
    normed = (
        mid_wide
        * lax.rsqrt(jnp.mean(mid_wide * mid_wide, axis=-1, keepdims=True) + EPSILON)
        * mixer_gain
    )
    normed = normed.astype(jnp.bfloat16)
    own_mid = lax.dynamic_slice_in_dim(mid, first_col, share_cols, 1)
    up_sums = jnp.dot(
        normed,
        lax.all_gather(up_weight, "sp", axis=0, tiled=True),
        preferred_element_type=jnp.float32,
    )
    hidden = jnp.square(jax.nn.relu(up_sums)).astype(jnp.bfloat16)
    down_part = jnp.dot(
        hidden,
        lax.all_gather(down_weight, "sp", axis=1, tiled=True),
        preferred_element_type=jnp.float32,
    )
    down_share = lax.psum_scatter(
        down_part.astype(jnp.bfloat16), "tp", scatter_dimension=1, tiled=True
    ).astype(jnp.float32)
    return (own_mid.astype(jnp.float32) + down_share).astype(jnp.bfloat16)


def solution(mesh):
    return jax.shard_map(
        shards,
        mesh=mesh,
        in_specs=(
            P("sp", "tp"),
            P("sp", "tp"),
            P("sp", "tp"),
            P(),
            P(),
            P("sp", None),
            P("tp", None),
            P(),
            P("sp", "tp"),
            P("tp", "sp"),
        ),
        out_specs=P("sp", "tp"),
        check_vma=False,
    )
```

profile of v0, /device:TPU:0, one launch (start us, length us, event | category | flops | bytes accessed | tf_op | source)
XLA Modules:
  0.0 400.8 jit_solution(354414603991874629)
XLA Ops:
  7.4 1.2 copy.18
  8.6 0.3 reshape.165
  8.9 0.1 bitcast_reduce_fusion.1
  9.0 0.9 copy.17
  10.1 0.8 mul.244
  10.8 0.1 broadcast_multiply_fusion.1
  10.9 0.1 fusion.28
  11.0 0.3 multiply_multiply_fusion
  11.3 0.7 subtract_convert_fusion
  12.0 0.6 pad_maximum_fusion
  12.6 0.1 convert_element_type.81
  12.7 0.8 mul.225
  13.5 0.1 multiply_multiply_fusion.1
  13.6 0.2 subtract_convert_fusion.1
  13.8 0.2 pad_maximum_fusion.1
  14.0 33.0 %all_gather.12 = bf16[2048,128]{0,1:T(8,128)(2,1)S(1)} all-gather(bf16[256,128]{0,1:T(8,128)(2,1)S(1)} %convert_element_type.79), channel_id=1, replica_groups=mesh['sp'=8,'tp'=4] {'sp'}, dimensions={0}, use_global_device_ids=true | all-gather | bytes 589824 | tf_op jit(solution)/shard_map/all_gather | solution.py:75
  47.0 8.1 %bitcast_reduce_fusion = (f32[2,4,256]{2,1,0:T(4,128)S(1)}, f32[2,2048,256,4]{2,1,3,0:T(8,128)}) fusion(bf16[2048,2,64,1]{0,2,3,1:T(8,128)(2,1)S(1)} %bitcast.63, bf16[256,2,4,64]{0,3,2,1:T(8,128)(2,1)S(1)} %convert_element_type.81), kind=kOutput, calls=%fused_computation.1 | convolution fusion | flops 545257472 | bytes 17571840 | tf_op jit(solution)/shard_map/while/body/eval_jaxpr/qhgd,khd->hgqk/dot_general | solution.py:40
  55.1 8.5 %fusion.1 = f32[2,4,256]{2,1,0:T(4,128)S(1)} fusion(f32[2,2048,256,4]{2,1,3,0:T(8,128)} %get-tuple-element.42, f32[2,4,256]{2,1,0:T(4,128)S(1)} %get-tuple-element.38), kind=kLoop, calls=%fused_computation.3 | loop fusion | flops 12580864 | bytes 16793600 | tf_op jit(solution)/shard_map/while/body/eval_jaxpr/reduce_sum | solution.py:45
  63.7 31.3 %all_gather.13 = bf16[2048,128]{1,0:T(8,128)(2,1)S(1)} all-gather(bf16[256,128]{1,0:T(8,128)(2,1)S(1)} %copy-done.1), channel_id=1, replica_groups=mesh['sp'=8,'tp'=4] {'sp'}, dimensions={0}, use_global_device_ids=true | all-gather | bytes 589824 | tf_op jit(solution)/shard_map/all_gather | solution.py:76
  95.0 0.2 copy.19
  95.2 7.4 %fusion.22 = bf16[256,2,4,64]{0,3,2,1:T(8,128)(2,1)S(1)} fusion(bf16[2048,2,64,1]{0,2,3,1:T(8,128)(2,1)S(1)} %bitcast.62, f32[2,2048,256,4]{2,1,3,0:T(8,128)} %get-tuple-element.42, f32[2,4,256]{2,1,0:T(4,128)S(1)} %get-tuple-element.38, f32[256,2,4]{0,2,1:T(4,128)S(1)} %bitcast_add_fusion, f32[256,2,4]{0,2,1:T(4,128)S(1)} %get-tuple-element.37), kind=kOutput, calls=%fused_computation.22 | convolution fusion | flops 549847040 | bytes 17588224 | tf_op jit(solution)/shard_map/while/body/eval_jaxpr/hgqk,khd->hgqd/dot_general | solution.py:46
  102.6 1.8 convolution_convert_fusion
  104.4 0.5 all-gather.3.cloned.1.call-update
  105.0 0.5 all-gather.5.cloned.1.call-update
  105.5 0.2 reduce-scatter.2.cloned.1.call-start
  105.8 36.5 %all-reduce.2.cloned.1.call-done = bf16[256,2048]{1,0:T(8,128)(2,1)} async-done(((bf16[256,2048]{1,0:T(8,128)(2,1)}), bf16[256,2048]{1,0:T(8,128)(2,1)}) %all-reduce.2.cloned.1.call-update) | async-done | bytes 1048592 | tf_op jit(solution)/shard_map/psum | solution.py:92
  142.3 2.1 fusion.7
  144.4 88.0 %all-gather.3.cloned.1.call-done = bf16[2048,2048]{1,0:T(8,128)(2,1)} async-done(((bf16[256,2048]{1,0:T(8,128)(2,1)}), bf16[2048,2048]{1,0:T(8,128)(2,1)}) %all-gather.3.cloned.1.call-update) | async-done | bytes 8388624 | tf_op jit(solution)/shard_map/all_gather | solution.py:104
  232.4 124.8 %all-gather.5.cloned.1.call-done = bf16[2048,2048]{1,0:T(8,128)(2,1)} async-done(((bf16[2048,256]{1,0:T(8,128)(2,1)}), bf16[2048,2048]{1,0:T(8,128)(2,1)}) %all-gather.5.cloned.1.call-update) | async-done | bytes 8388624 | tf_op jit(solution)/shard_map/all_gather | solution.py:110
  357.2 11.3 %convolution_convert_fusion.1 = bf16[256,2048]{1,0:T(8,128)(2,1)} fusion(bf16[2048,2048]{1,0:T(8,128)(2,1)} %all-gather.5.cloned.1.call-done, bf16[2048,2048]{1,0:T(8,128)(2,1)} %all-gather.3.cloned.1.call-done, bf16[256,2048]{1,0:T(8,128)(2,1)S(1)} %get-tuple-element.20, f32[2048]{0:T(1024)S(1)} %copy-done.2, f32[256]{0:T(256)S(1)} %add_rsqrt_fusion.2), kind=kOutput, calls=%fused_computation.12 | convolution fusion | flops 4299161600 | bytes 18883584 | tf_op jit(solution)/shard_map/dot_general | solution.py:108
  368.5 23.1 %reduce-scatter.2.cloned.1.call-done = bf16[256,512]{1,0:T(8,128)(2,1)} async-done(((bf16[256,2048]{1,0:T(8,128)(2,1)}), bf16[256,512]{1,0:T(8,128)(2,1)}) %reduce-scatter.2.cloned.1.call-update) | async-done | bytes 262160 | tf_op jit(solution)/shard_map/reduce_scatter | solution.py:113
  391.6 1.7 add_convert_fusion.1
  (21 shorter events, 0.3 us)
Async XLA Ops:
  7.4 95.2 %copy-start = (bf16[512,2048]{1,0:T(8,128)(2,1)S(1)}, bf16[512,2048]{1,0:T(8,128)(2,1)}, u32[]{:S(2)}) copy-start(bf16[512,2048]{1,0:T(8,128)(2,1)} %param.16) | copy-start | bytes 6291460
  7.4 134.9 %all-reduce.2.cloned.1.call-start = ((), (), s32[]{:S(2)}) async-start(), calls=%async_computation.1 | async-start | bytes 2097152 | tf_op jit(solution)/shard_map/psum | solution.py:92
  55.1 8.6 %copy-start.1 = (bf16[256,128]{1,0:T(8,128)(2,1)S(1)}, bf16[256,128]{1,0:T(8,128)(2,1)}, u32[]{:S(2)}) copy-start(bf16[256,128]{1,0:T(8,128)(2,1)} %param.12) | copy-start | bytes 196612
  102.6 254.6 %copy-start.2 = (f32[2048]{0:T(1024)S(1)}, f32[2048]{0:T(1024)}, u32[]{:S(2)}) copy-start(f32[2048]{0:T(1024)} %param.17) | copy-start | bytes 24580
  104.4 128.0 %all-gather.3.cloned.1.call-start = ((), (), s32[]{:S(2)}) async-start(), calls=%async_computation.2 | async-start | bytes 9437184 | tf_op jit(solution)/shard_map/all_gather | solution.py:104
  104.9 252.3 %all-gather.5.cloned.1.call-start = ((), (), s32[]{:S(2)}) async-start(), calls=%async_computation.3 | async-start | bytes 9437184 | tf_op jit(solution)/shard_map/all_gather | solution.py:110
  105.5 286.1 %reduce-scatter.2.cloned.1.call-start = ((), (), s32[]{:S(2)}) async-start(), calls=%async_computation.4 | async-start | bytes 1310720 | tf_op jit(solution)/shard_map/reduce_scatter | solution.py:113
Sparse Core Ops, SparseCore 0:
  104.5 37.7 all-reduce.1
  368.6 22.9 reduce-scatter.1
Sparse Core Ops, SparseCore 1:
  107.0 125.3 all-gather.2
  234.3 122.9 all-gather.4
where the time goes:
time: 401 us
  waiting for transfers between devices  274 us (68%)
  blocking collectives  64.3 us (16%)
  matrix products  28.5 us (7%)
  between operations  15.1 us (4%)
  other arithmetic  14.7 us (4%)
  local copies, waits for them, and re-layouts  4.36 us (1%)
    all_gather x1, waiting for transfers between devices, shards(): lax.all_gather(down_weight, 'sp', axis=1, tiled=True)  125 us
    all_gather x1, waiting for transfers between devices, shards(): lax.all_gather(up_weight, 'sp', axis=0, tiled=True)  88 us
    psum x1, waiting for transfers between devices, shards(): lax.psum(partial_value.astype(jnp.bfloat16), 'tp').astype(jnp.float32)  36.5 us
    all_gather x1, blocking collectives, shards(): key_rows = lax.all_gather(prepared_keys, 'sp', axis=0, tiled=True)  33 us
    all_gather x1, blocking collectives, shards(): value_rows = lax.all_gather(values, 'sp', axis=0, tiled=True)  31.3 us
    reduce_scatter x1, waiting for transfers between devices, shards(): lax.psum_scatter(down_part.astype(jnp.bfloat16), 'tp', scatter_dimension=...  23.1 us
    dot_general x1, matrix products, shards(): jnp.dot(hidden, lax.all_gather(down_weight, 'sp', axis=1, tiled=True), pr...  11.3 us
    reduce_sum x1, other arithmetic, attend_block(): totals = totals * rescale + jnp.sum(exps, axis=-1)  8.52 us
  transfers between devices with their start and end apart: 4, of which 4 were waited for; matrix products, arithmetic and copies ran while one was open for 1% of the time, Pallas kernels for 0%

commit v1 on v0

--- a/solution.py
+++ b/solution.py
@@ -89,7 +89,9 @@
     model_width = partial_value.shape[1]
     share_cols = model_width // lax.axis_size("tp")
     first_col = lax.axis_index("tp") * share_cols
-    summed = lax.psum(partial_value.astype(jnp.bfloat16), "tp").astype(jnp.float32)
+    summed = jnp.sum(lax.all_gather(partial_value.astype(jnp.bfloat16), "tp"), axis=0).astype(
+        jnp.float32
+    )
     mid = (stream.astype(jnp.float32) + summed).astype(jnp.bfloat16)
     mid_wide = mid.astype(jnp.float32)
     normed = (

time: 401 us -> 435 us (1.085)
  waiting for transfers between devices: 274 us -> 305 us
    psum x1 -> x0, waiting for transfers between devices: 36.5 us -> none  [shards(): lax.psum(partial_value.astype(jnp.bfloat16), 'tp').astype(jnp.float32)]
    all_gather x0 -> x1, waiting for transfers between devices: none -> 34.1 us  [shards(): lax.all_gather(partial_value.astype(jnp.bfloat16), 'tp')]
    all_gather x1, waiting for transfers between devices: 88 us -> 121 us  [shards(): lax.all_gather(up_weight, 'sp', axis=0, tiled=True)]
where the time goes in v1:
time: 435 us; the launch traced here: 434 us
  waiting for transfers between devices  305 us (70%)
  blocking collectives  64.3 us (15%)
  matrix products  28.8 us (7%)
  other arithmetic  18.3 us (4%)
  between operations  13.3 us (3%)
  local copies, waits for them, and re-layouts  4.36 us (1%)
    all_gather x1, waiting for transfers between devices, shards(): lax.all_gather(down_weight, 'sp', axis=1, tiled=True)  125 us
    all_gather x1, waiting for transfers between devices, shards(): lax.all_gather(up_weight, 'sp', axis=0, tiled=True)  121 us
    all_gather x1, waiting for transfers between devices, shards(): lax.all_gather(partial_value.astype(jnp.bfloat16), 'tp')  34.1 us
    all_gather x1, blocking collectives, shards(): key_rows = lax.all_gather(prepared_keys, 'sp', axis=0, tiled=True)  33 us
    all_gather x1, blocking collectives, shards(): value_rows = lax.all_gather(values, 'sp', axis=0, tiled=True)  31.3 us
    reduce_scatter x1, waiting for transfers between devices, shards(): lax.psum_scatter(down_part.astype(jnp.bfloat16), 'tp', scatter_dimension=...  23.1 us
    dot_general x1, matrix products, shards(): jnp.dot(hidden, lax.all_gather(down_weight, 'sp', axis=1, tiled=True), pr...  11.6 us
  transfers between devices with their start and end apart: 4, of which 4 were waited for; matrix products, arithmetic and copies ran while one was open for 1% of the time, Pallas kernels for 0%

profile of v1, /device:TPU:0, one launch (start us, length us, event | category | flops | bytes accessed | tf_op | source)
XLA Modules:
  0.0 434.2 jit_solution(17631543963495231398)
XLA Ops:
  6.6 1.2 copy.18
  7.8 0.3 reshape.165
  8.1 0.9 copy.17
  9.2 0.8 mul.244
  10.0 0.1 broadcast_multiply_fusion.1
  10.1 0.1 fusion.28
  10.2 0.3 multiply_multiply_fusion
  10.5 0.7 subtract_convert_fusion
  11.1 0.6 pad_maximum_fusion
  11.7 0.1 convert_element_type.83
  11.9 0.8 mul.225
  12.6 0.1 multiply_multiply_fusion.1
  12.7 0.2 subtract_convert_fusion.1
  12.9 0.2 pad_maximum_fusion.1
  13.1 33.0 %all_gather.18 = bf16[2048,128]{0,1:T(8,128)(2,1)S(1)} all-gather(bf16[256,128]{0,1:T(8,128)(2,1)S(1)} %convert_element_type.81), channel_id=1, replica_groups=mesh['sp'=8,'tp'=4] {'sp'}, dimensions={0}, use_global_device_ids=true | all-gather | bytes 589824 | tf_op jit(solution)/shard_map/all_gather | solution.py:75
  46.2 8.1 %bitcast_reduce_fusion = (f32[2,4,256]{2,1,0:T(4,128)S(1)}, f32[2,2048,256,4]{2,1,3,0:T(8,128)}) fusion(bf16[2048,2,64,1]{0,2,3,1:T(8,128)(2,1)S(1)} %bitcast.65, bf16[256,2,4,64]{0,3,2,1:T(8,128)(2,1)S(1)} %convert_element_type.83), kind=kOutput, calls=%fused_computation.1 | convolution fusion | flops 545257472 | bytes 17571840 | tf_op jit(solution)/shard_map/while/body/eval_jaxpr/qhgd,khd->hgqk/dot_general | solution.py:40
  54.3 8.5 %fusion.1 = f32[2,4,256]{2,1,0:T(4,128)S(1)} fusion(f32[2,2048,256,4]{2,1,3,0:T(8,128)} %get-tuple-element.42, f32[2,4,256]{2,1,0:T(4,128)S(1)} %get-tuple-element.38), kind=kLoop, calls=%fused_computation.3 | loop fusion | flops 12580864 | bytes 16793600 | tf_op jit(solution)/shard_map/while/body/eval_jaxpr/reduce_sum | solution.py:45
  62.9 31.3 %all_gather.19 = bf16[2048,128]{1,0:T(8,128)(2,1)S(1)} all-gather(bf16[256,128]{1,0:T(8,128)(2,1)S(1)} %copy-done.1), channel_id=1, replica_groups=mesh['sp'=8,'tp'=4] {'sp'}, dimensions={0}, use_global_device_ids=true | all-gather | bytes 589824 | tf_op jit(solution)/shard_map/all_gather | solution.py:76
  94.1 0.2 copy.19
  94.4 7.4 %fusion.22 = bf16[256,2,4,64]{0,3,2,1:T(8,128)(2,1)S(1)} fusion(bf16[2048,2,64,1]{0,2,3,1:T(8,128)(2,1)S(1)} %bitcast.64, f32[2,2048,256,4]{2,1,3,0:T(8,128)} %get-tuple-element.42, f32[2,4,256]{2,1,0:T(4,128)S(1)} %get-tuple-element.38, f32[256,2,4]{0,2,1:T(4,128)S(1)} %bitcast_add_fusion, f32[256,2,4]{0,2,1:T(4,128)S(1)} %get-tuple-element.37), kind=kOutput, calls=%fused_computation.22 | convolution fusion | flops 549847040 | bytes 17588224 | tf_op jit(solution)/shard_map/while/body/eval_jaxpr/hgqk,khd->hgqd/dot_general | solution.py:46
  101.7 1.7 convolution_convert_fusion
  103.5 0.7 all-gather.5.cloned.1.call-update
  104.3 0.7 all-gather.7.cloned.1.call-update
  105.0 0.2 reduce-scatter.2.cloned.1.call-start
  105.2 34.1 %all-gather.9.cloned.1.call-done = bf16[1024,2048]{1,0:T(8,128)(2,1)} async-done(((bf16[256,2048]{1,0:T(8,128)(2,1)}), bf16[1024,2048]{1,0:T(8,128)(2,1)}) %all-gather.9.cloned.1.call-update) | async-done | bytes 4194320 | tf_op jit(solution)/shard_map/all_gather | solution.py:92
  139.3 3.1 reduce_sum.55
  142.4 2.6 fusion.7
  145.0 121.0 %all-gather.5.cloned.1.call-done = bf16[2048,2048]{1,0:T(8,128)(2,1)} async-done(((bf16[256,2048]{1,0:T(8,128)(2,1)}), bf16[2048,2048]{1,0:T(8,128)(2,1)}) %all-gather.5.cloned.1.call-update) | async-done | bytes 8388624 | tf_op jit(solution)/shard_map/all_gather | solution.py:106
  265.9 125.2 %all-gather.7.cloned.1.call-done = bf16[2048,2048]{1,0:T(8,128)(2,1)} async-done(((bf16[2048,256]{1,0:T(8,128)(2,1)}), bf16[2048,2048]{1,0:T(8,128)(2,1)}) %all-gather.7.cloned.1.call-update) | async-done | bytes 8388624 | tf_op jit(solution)/shard_map/all_gather | solution.py:112
  391.1 11.6 %convolution_convert_fusion.1 = bf16[256,2048]{1,0:T(8,128)(2,1)} fusion(bf16[2048,2048]{1,0:T(8,128)(2,1)} %all-gather.7.cloned.1.call-done, bf16[2048,2048]{1,0:T(8,128)(2,1)} %all-gather.5.cloned.1.call-done, bf16[256,2048]{1,0:T(8,128)(2,1)} %get-tuple-element.20, f32[2048]{0:T(1024)S(1)} %copy-done.2, f32[256]{0:T(256)S(1)} %add_rsqrt_fusion.2), kind=kOutput, calls=%fused_computation.12 | convolution fusion | flops 4299161600 | bytes 18883584 | tf_op jit(solution)/shard_map/dot_general | solution.py:110
  402.8 23.1 %reduce-scatter.2.cloned.1.call-done = bf16[256,512]{1,0:T(8,128)(2,1)} async-done(((bf16[256,2048]{1,0:T(8,128)(2,1)}), bf16[256,512]{1,0:T(8,128)(2,1)}) %reduce-scatter.2.cloned.1.call-update) | async-done | bytes 262160 | tf_op jit(solution)/shard_map/reduce_scatter | solution.py:115
  425.9 1.8 add_convert_fusion.1
  (22 shorter events, 0.4 us)
Async XLA Ops:
  6.5 95.2 %copy-start = (bf16[512,2048]{1,0:T(8,128)(2,1)S(1)}, bf16[512,2048]{1,0:T(8,128)(2,1)}, u32[]{:S(2)}) copy-start(bf16[512,2048]{1,0:T(8,128)(2,1)} %param.16) | copy-start | bytes 6291460
  6.5 132.8 %all-gather.9.cloned.1.call-start = ((), (), s32[]{:S(2)}) async-start(), calls=%async_computation.4 | async-start | bytes 5242880 | tf_op jit(solution)/shard_map/all_gather | solution.py:92
  54.3 8.6 %copy-start.1 = (bf16[256,128]{1,0:T(8,128)(2,1)S(1)}, bf16[256,128]{1,0:T(8,128)(2,1)}, u32[]{:S(2)}) copy-start(bf16[256,128]{1,0:T(8,128)(2,1)} %param.12) | copy-start | bytes 196612
  101.7 289.4 %copy-start.2 = (f32[2048]{0:T(1024)S(1)}, f32[2048]{0:T(1024)}, u32[]{:S(2)}) copy-start(f32[2048]{0:T(1024)} %param.17) | copy-start | bytes 24580
  103.5 162.4 %all-gather.5.cloned.1.call-start = ((), (), s32[]{:S(2)}) async-start(), calls=%async_computation.1 | async-start | bytes 9437184 | tf_op jit(solution)/shard_map/all_gather | solution.py:106
  104.2 286.9 %all-gather.7.cloned.1.call-start = ((), (), s32[]{:S(2)}) async-start(), calls=%async_computation.2 | async-start | bytes 9437184 | tf_op jit(solution)/shard_map/all_gather | solution.py:112
  105.0 320.9 %reduce-scatter.2.cloned.1.call-start = ((), (), s32[]{:S(2)}) async-start(), calls=%async_computation.3 | async-start | bytes 1310720 | tf_op jit(solution)/shard_map/reduce_scatter | solution.py:115
Sparse Core Ops, SparseCore 0:
  103.6 35.6 all-gather.8
  141.4 124.4 all-gather.4
  268.0 123.1 all-gather.6
  402.9 22.9 reduce-scatter.1
